TPU v7x, 512 devices: a whole 4x8x8 slice. The times are simulated.
512 devices in a mesh: sp: 32 (over z, x), tp: 16 (over y, core).
Axes of the slice: x: 4, y: 8, z: 8, core: 2. Of those that a mesh axis runs over, the one named last changes fastest.
Arguments:
- residual: bfloat16 [8192, 2048], P('sp', 'tp'), may hold values from -26 to 26
- queries: bfloat16 [2048, 8192], P('tp', 'sp'), may hold values from -6 to 6
- keys: bfloat16 [2048, 8192], P('tp', 'sp'), may hold values from -6 to 6
- values: bfloat16 [2048, 8192], P('tp', 'sp'), may hold values from -12 to 12
- forget_cache: float32 [32, 8192], P('tp', 'sp'), as said below
- out_weight: bfloat16 [2048, 2048], P('tp'), may hold values from -0.125 to 0.125
- norm_gain: float32 [2048], replicated, may hold values from 0.1 to 1.9
- routes: int32 [8192, 2], P('sp'), may hold values from 0 to 31, all different within a row; in each aligned block of 256 rows (0 to 255, 256 to 511, ...) at most 20 rows name the same one
- route_weight: float32 [8192, 2], P('sp'), may hold values from 0.2 to 1
- gate_weight: bfloat16 [32, 2048, 4096], P('sp', None, 'tp'), may hold values from -0.125 to 0.125
- up_weight: bfloat16 [32, 2048, 4096], P('sp', None, 'tp'), may hold values from -0.125 to 0.125
- down_weight: bfloat16 [32, 4096, 2048], P('sp', 'tp'), may hold values from -0.09375 to 0.09375
Outputs:
- updated: bfloat16 [8192, 2048], P('sp', 'tp')
Inputs may be any that keep to these rules, and one draw needn't show every extreme that they name: `routes`: each row names 2 different experts; within the 256 rows of one index of sp no expert is named by more than 20 rows, and in the rows of some index some expert is named by exactly 20. `forget_cache`: each head's row never rises from one position to the next.
All inputs are finite; a program needn't handle non-finite values.
Results may differ from a plain program's by a relative error of at most 0.013.
Values may be sent and summed in bfloat16 or wider, within the bound.
No kernel may reach another device: no remote copies, remote signals or barrier semaphores. Data moves between devices by JAX's collectives and lax.ppermute only.
A program may use at most 64 MiB of HBM per device.

v0:
```python
import jax
import jax.numpy as jnp
from jax import lax
from jax.sharding import Mesh
from jax.sharding import PartitionSpec as P

SP = ("sp_0", "sp_1")
norm_eps = 1e-06
masked_score = -1e30
key_span = 1024


def gathered_by_axis(shard, axes, dim):
    out = shard
    for number in range(len(axes) - 1, -1, -1):
        out = lax.all_gather(out, axes[number], axis=dim, tiled=True)
    return out


def cut_along(shard, dim, peers):
    before, after = (shard.shape[:dim], shard.shape[dim + 1 :])
    return jnp.moveaxis(shard.reshape(*before, peers, -1, *after), dim, 0)


def sum_at_owner(shard, axis, dim):
    peers = lax.axis_size(axis)
    pieces = lax.all_to_all(cut_along(shard, dim, peers), axis, 0, 0, tiled=True)
    return jnp.sum(pieces.astype(jnp.float32), axis=0)


def sent_to_all(shard, axis):
    copies = jnp.broadcast_to(shard, (lax.axis_size(axis), *shard.shape))
    return lax.all_to_all(copies, axis, split_axis=0, concat_axis=0, tiled=True)


def taken_together(shard, axis):
    return sent_to_all(shard, axis).sum(axis=0)


def shards(
    residual,
    queries,
    keys,
    values,
    forget_cache,
    out_weight,
    norm_gain,
    routes,
    route_weight,
    gate_weight,
    up_weight,
    down_weight,
):
    sp_count = lax.axis_size(SP)
    token_count, local_width = residual.shape
    model_width = norm_gain.shape[0]
    head_count = forget_cache.shape[0]
    head_width = queries.shape[0] // head_count
    first_token = lax.axis_index(SP) * token_count
    last_token = first_token + token_count - 1
    query_heads = queries.reshape(head_count, head_width, token_count)
    query_place = first_token + jnp.arange(token_count, dtype=jnp.int32)
    score_scale = head_width ** (-0.5)

    def attend_block(state_now, key_block, value_block, cache_block, key_first):
        running_peak, running_total, running_sum = state_now
        block_length = key_block.shape[1]
        key_heads = key_block.reshape(head_count, head_width, block_length)
        value_heads = value_block.reshape(head_count, head_width, block_length)
        scores = (
            jnp.einsum("hdq,hdk->hqk", query_heads, key_heads, preferred_element_type=jnp.float32)
            * score_scale
        )
        scores = scores + forget_cache[:, :, None] - cache_block[:, None, :]
        key_place = key_first + jnp.arange(block_length, dtype=jnp.int32)
        allowed = key_place[None, :] <= query_place[:, None]
        scores = jnp.where(allowed[None], scores, masked_score)
        new_peak = jnp.maximum(running_peak, jnp.max(scores, axis=2))
        weights = jnp.exp(scores - new_peak[:, :, None])
        shrink = jnp.exp(running_peak - new_peak)
        new_total = running_total * shrink + jnp.sum(weights, axis=2)
        new_sum = running_sum * shrink[:, None, :] + jnp.einsum(
            "hdk,hqk->hdq",
            value_heads,
            weights.astype(jnp.bfloat16),
            preferred_element_type=jnp.float32,
        )
        return (new_peak, new_total, new_sum)

    initial = (
        jnp.full((head_count, token_count), masked_score, jnp.float32),
        jnp.zeros((head_count, token_count), jnp.float32),
        jnp.zeros((head_count, head_width, token_count), jnp.float32),
    )
    key_part = gathered_by_axis(keys.astype(jnp.float32), SP, 1).astype(jnp.bfloat16)
    value_part = gathered_by_axis(values.astype(jnp.float32), SP, 1).astype(jnp.bfloat16)
    cache_part = gathered_by_axis(forget_cache, SP, 1)
    part_length = key_part.shape[1]
    block_length = key_span

    def one_block(block_index, state_in):
        start_column = block_index * block_length
        key_block = lax.dynamic_slice_in_dim(key_part, start_column, block_length, 1)
        value_block = lax.dynamic_slice_in_dim(value_part, start_column, block_length, 1)
        cache_block = lax.dynamic_slice_in_dim(cache_part, start_column, block_length, 1)
        return lax.cond(
            start_column <= last_token,
            lambda inner: attend_block(inner, key_block, value_block, cache_block, start_column),
            lambda inner: inner,
            state_in,
        )

    final_peak, final_total, final_sum = lax.fori_loop(
        0, part_length // block_length, one_block, initial
    )
    attended = (
        (final_sum / final_total[:, None, :])
        .astype(jnp.bfloat16)
        .reshape(head_count * head_width, token_count)
    )
    projected = lax.dot_general(
        attended, out_weight, (((0,), (0,)), ((), ())), preferred_element_type=jnp.float32
    )
    head_sum = sum_at_owner(projected.astype(jnp.bfloat16), "tp", 1)
    stream = (residual.astype(jnp.float32) + head_sum).astype(jnp.bfloat16)
    top_count = routes.shape[1]
    item_count = token_count * top_count
    capacity = max(2, token_count * top_count * 5 // (4 * sp_count))
    expert_of = routes.reshape(item_count)
    onehot = (expert_of[:, None] == jnp.arange(sp_count, dtype=jnp.int32)[None, :]).astype(
        jnp.int32
    )
    earlier = jnp.cumsum(onehot, axis=0) - onehot
    target = expert_of * capacity + jnp.sum(earlier * onehot, axis=1)
    matches = target[None, :] == jnp.arange(sp_count * capacity, dtype=jnp.int32)[:, None]
    filled = jnp.any(matches, axis=1)
    source_row = (
        jnp.sum(jnp.where(matches, jnp.arange(item_count, dtype=jnp.int32)[None, :], 0), axis=1)
        // top_count
    )
    local_rows = stream.astype(jnp.float32)
    squares = taken_together(jnp.sum(local_rows * local_rows, axis=1), "tp")
    row_scale = lax.rsqrt(squares / model_width + norm_eps)
    local_gain = lax.dynamic_slice_in_dim(
        norm_gain, lax.axis_index("tp") * local_width, local_width
    )
    normed = (local_rows * row_scale[:, None] * local_gain[None, :]).astype(jnp.bfloat16)
    taken_rows = jnp.take(normed, source_row, axis=0)
    taken_rows = jnp.where(filled[:, None], taken_rows, jnp.zeros((), normed.dtype))
    arrived = lax.all_gather(
        lax.all_to_all(
            taken_rows.reshape(sp_count, capacity, normed.shape[1]),
            SP,
            split_axis=0,
            concat_axis=0,
            tiled=True,
        ),
        "tp",
        axis=2,
        tiled=True,
    )
    source_count = arrived.shape[0]
    slot_count = arrived.shape[1]
    flat_rows = arrived.reshape(source_count * slot_count, model_width)
    gate_value = jnp.dot(flat_rows, gate_weight[0], preferred_element_type=jnp.float32)
    up_value = jnp.dot(flat_rows, up_weight[0], preferred_element_type=jnp.float32)
    hidden = (jax.nn.silu(gate_value) * up_value).astype(jnp.bfloat16)
    down_value = jnp.dot(hidden, down_weight[0], preferred_element_type=jnp.float32)
    summed = sum_at_owner(
        down_value.reshape(source_count, slot_count, model_width).astype(jnp.bfloat16), "tp", 2
    )
    expert_back = lax.all_to_all(
        summed.astype(jnp.bfloat16), SP, split_axis=0, concat_axis=0, tiled=True
    )
    back_rows = expert_back.reshape(sp_count * capacity, local_width)
    picked = (
        jnp.take(back_rows, target, axis=0).astype(jnp.float32)
        * route_weight.reshape(item_count)[:, None]
    )
    mixture = jnp.sum(picked.reshape(token_count, top_count, local_width), axis=1)
    return (stream.astype(jnp.float32) + mixture).astype(jnp.bfloat16)


def solution(mesh):
    finer = Mesh(mesh.devices.reshape(8, 4, mesh.shape["tp"]), ("sp_0", "sp_1", "tp"))
    in_specs = (
        P(SP, "tp"),
        P("tp", SP),
        P("tp", SP),
        P("tp", SP),
        P("tp", SP),
        P("tp", None),
        P(),
        P(SP, None),
        P(SP, None),
        P(SP, None, "tp"),
        P(SP, None, "tp"),
        P(SP, "tp", None),
    )
    out_specs = P(SP, "tp")
    return jax.shard_map(
        shards, mesh=finer, in_specs=in_specs, out_specs=out_specs, check_vma=False
    )
```

profile of v0, /device:TPU:24, one launch (start us, length us, event | category | flops | bytes accessed | tf_op | source)
XLA Modules:
  0.0 361.6 jit_solution(1007863958048043251)
XLA Ops:
  6.5 14.3 %all_gather.21 = bf16[128,1024]{1,0:T(8,128)(2,1)} all-gather(bf16[128,256]{1,0:T(8,128)(2,1)} %param.18), channel_id=1, replica_groups=mesh['sp_0'=8,'sp_1'=4,'tp'=16] {'sp_1'}, dimensions={1}, use_global_device_ids=true | all-gather | bytes 327680 | tf_op jit(solution)/shard_map/all_gather | solution.py:16
  20.9 13.2 %all_gather.25 = bf16[128,1024]{1,0:T(8,128)(2,1)} all-gather(bf16[128,256]{1,0:T(8,128)(2,1)} %param.19), channel_id=1, replica_groups=mesh['sp_0'=8,'sp_1'=4,'tp'=16] {'sp_1'}, dimensions={1}, use_global_device_ids=true | all-gather | bytes 327680 | tf_op jit(solution)/shard_map/all_gather | solution.py:16
  34.2 10.6 %all_gather.23 = f32[2,1024]{1,0:T(2,128)S(1)} all-gather(f32[2,256]{1,0:T(2,128)} %param.20), channel_id=1, replica_groups=mesh['sp_0'=8,'sp_1'=4,'tp'=16] {'sp_1'}, dimensions={1}, use_global_device_ids=true | all-gather | bytes 10240 | tf_op jit(solution)/shard_map/all_gather | solution.py:16
  44.8 31.0 %all_gather.24 = f32[2,8192]{1,0:T(2,128)S(1)} all-gather(f32[2,1024]{1,0:T(2,128)S(1)} %all_gather.23), channel_id=1, replica_groups=mesh['sp_0'=8,'sp_1'=4,'tp'=16] {'sp_0'}, dimensions={1}, use_global_device_ids=true | all-gather | bytes 73728 | tf_op jit(solution)/shard_map/all_gather | solution.py:16
  75.7 36.7 %all-gather.6.cloned.1.call-done = bf16[128,8192]{1,0:T(8,128)(2,1)} async-done(((bf16[128,1024]{1,0:T(8,128)(2,1)}), bf16[128,8192]{1,0:T(8,128)(2,1)}) %all-gather.6.cloned.1.call-update) | async-done | bytes 2097168 | tf_op jit(solution)/shard_map/all_gather | solution.py:16
  112.5 4.2 %while.18 = (s32[]{:T(128)}, f32[2,256]{1,0:T(2,128)S(1)}, f32[2,256]{1,0:T(2,128)S(1)}, f32[2,64,256]{2,1,0:T(8,128)S(1)}, s32[]{:T(128)}, /*index=5*/bf16[128,...) while((s32[]{:T(128)}, f32[2,256]{1,0:T(2,128)S(1)}, ...), condition=%wide.region_5.6_spmd.clone, body=%wide.region_0.5_spmd.clone.sunk | while | flops 139266304 | bytes 8788313 | solution.py:113
  112.5 3.8 %conditional.3 = ((f32[2,256]{1,0:T(2,128)S(1)}, f32[2,256]{1,0:T(2,128)S(1)}, f32[2,64,256]{2,1,0:T(8,128)S(1)})) conditional(s32[]{:T(128)} %convert_element_type.119, (f32[2,256]{1,0:T(2,128)S(1)}, f32[2,256]{1,0:T(2,128)S(1)}, f32[2,64,256]{2,1,0:T(8,128)S(1)}) %tuple.55, (s32[]{:T(128)}, s32[]{:T(128)}, bf16[128,8192]{1,0:T(8,128)(2,1)}, ...), branch_computations={%region_1.0_spmd, %region_2.4_spmd} | conditional | flops 139266304 | bytes 8787026 | solution.py:106
  112.5 1.1 constant_dynamic-slice_fusion
  113.7 0.2 broadcast_compare_fusion
  113.9 1.6 fusion.26
  115.5 0.3 fusion.3
  115.8 0.5 convolution_add_fusion
  116.7 0.5 fusion.7
  117.2 1.3 copy.95
  118.4 7.4 %all-to-all-start = ((bf16[16,256,128]{2,1,0:T(8,128)(2,1)}), bf16[16,256,128]{2,1,0:T(8,128)(2,1)S(1)}, u32[]{:S(2)}, u32[]{:S(2)}) async-start(bf16[16,256,128]{2,1,0:T(8,128)(2,1)} %bitcast.60), calls=%async_computation | async-start | bytes 2097152 | tf_op jit(solution)/shard_map/all_to_all | solution.py:27
  126.0 0.1 eq.39
  126.1 0.1 reshape.233
  126.3 1.2 reduce-window.6
  127.4 0.2 slice_reduce_fusion
  127.8 0.2 select_reduce_fusion
  128.2 0.2 fusion.8
  128.4 23.6 %all-to-all-done = bf16[16,256,128]{2,1,0:T(8,128)(2,1)S(1)} async-done(((bf16[16,256,128]{2,1,0:T(8,128)(2,1)}), bf16[16,256,128]{2,1,0:T(8,128)(2,1)S(1)}, u32[]{:S(2)}, u32[]{:S(2)}) %all-to-all-start) | async-done | bytes 1048608 | tf_op jit(solution)/shard_map/all_to_all | solution.py:27
  152.0 0.1 convert_reduce_fusion
  152.3 0.6 broadcast_in_dim.101
  152.9 5.2 %all-to-all-start.1 = ((f32[16,1,256]{2,1,0:T(1,128)}), f32[16,1,256]{2,1,0:T(1,128)S(1)}, u32[]{:S(2)}, u32[]{:S(2)}) async-start(f32[16,1,256]{2,1,0:T(1,128)} %broadcast_in_dim.101), calls=%async_computation.1 | async-start | bytes 32768 | tf_op jit(solution)/shard_map/all_to_all | solution.py:33
  158.3 0.8 dynamic_slice.42
  159.1 3.6 all-to-all-done.1
  162.8 2.0 gather_fusion
  164.8 0.3 select_select_fusion
  165.1 44.1 %all_to_all.26 = bf16[32,20,128]{2,1,0:T(8,128)(2,1)} all-to-all(bf16[32,20,128]{2,1,0:T(8,128)(2,1)S(1)} %select_select_fusion), channel_id=1, replica_groups=mesh['sp_0'=8,'sp_1'=4,'tp'=16] {'sp_0','sp_1'}, dimensions={0} | all-to-all | bytes 327680 | tf_op jit(solution)/shard_map/all_to_all | solution.py:151
  209.2 39.2 %all-gather.8.cloned.1.call-done = bf16[32,20,2048]{2,1,0:T(8,128)(2,1)} async-done(((bf16[32,20,128]{2,1,0:T(8,128)(2,1)}), bf16[32,20,2048]{2,1,0:T(8,128)(2,1)}) %all-gather.8.cloned.1.call-update) | async-done | bytes 2621456 | tf_op jit(solution)/shard_map/all_gather | solution.py:150
  248.5 5.2 %reshape.235 = bf16[640,2048]{1,0:T(8,128)(2,1)} reshape(bf16[32,20,2048]{2,1,0:T(8,128)(2,1)} %all-gather.8.cloned.1.call-done) | data formatting | bytes 5242880 | tf_op jit(solution)/shard_map/reshape | solution.py:164
  253.7 2.7 fusion.12
  256.5 0.8 fusion.9
  257.4 0.9 fusion.6
  258.3 2.2 copy.94
  260.5 6.4 %all-to-all-start.3 = ((bf16[16,32,20,128]{3,1,2,0:T(8,128)(2,1)}), bf16[16,32,20,128]{3,1,2,0:T(8,128)(2,1)}, u32[]{:S(2)}, u32[]{:S(2)}) async-start(bf16[16,32,20,128]{3,1,2,0:T(8,128)(2,1)} %bitcast.62), calls=%async_computation.3 | async-start | bytes 5242880 | tf_op jit(solution)/shard_map/all_to_all | solution.py:27
  266.9 0.1 reduce_sum.88
  267.2 0.1 mul.123
  267.4 0.2 copy.75
  267.8 59.1 %all-to-all-done.3 = bf16[16,32,20,128]{3,1,2,0:T(8,128)(2,1)} async-done(((bf16[16,32,20,128]{3,1,2,0:T(8,128)(2,1)}), bf16[16,32,20,128]{3,1,2,0:T(8,128)(2,1)}, u32[]{:S(2)}, u32[]{:S(2)}) %all-to-all-start.3) | async-done | bytes 2621472 | tf_op jit(solution)/shard_map/all_to_all | solution.py:27
  326.9 2.1 reduce_sum.94
  329.0 0.7 copy.80
  329.8 9.9 %all-to-all-start.4 = ((bf16[32,20,128]{2,1,0:T(8,128)(2,1)}), bf16[32,20,128]{2,1,0:T(8,128)(2,1)S(1)}, u32[]{:S(2)}, u32[]{:S(2)}) async-start(bf16[32,20,128]{2,1,0:T(8,128)(2,1)} %copy.80), calls=%async_computation.4 | async-start | bytes 393216 | tf_op jit(solution)/shard_map/all_to_all | solution.py:172
  339.7 11.8 %all-to-all-done.4 = bf16[32,20,128]{2,1,0:T(8,128)(2,1)S(1)} async-done(((bf16[32,20,128]{2,1,0:T(8,128)(2,1)}), bf16[32,20,128]{2,1,0:T(8,128)(2,1)S(1)}, u32[]{:S(2)}, u32[]{:S(2)}) %all-to-all-start.4) | async-done | bytes 163872 | tf_op jit(solution)/shard_map/all_to_all | solution.py:172
  351.6 1.3 gather_fusion.1
  353.0 1.5 multiply_reduce_fusion
  354.4 0.7 fusion.18
  (73 shorter events, 1.7 us)
Async XLA Ops:
  6.5 250.9 %copy-start = (bf16[1,256,2048]{2,1,0:T(8,128)(2,1)S(1)}, bf16[1,256,2048]{2,1,0:T(8,128)(2,1)}, u32[]{:S(2)}) copy-start(bf16[1,256,2048]{2,1,0:T(8,128)(2,1)} %param.27) | copy-start | bytes 3145732
  6.5 69.2 %all-gather.4.cloned.1.call-start = ((), (), s32[]{:S(2)}) async-start(), calls=%async_computation.5 | async-start | bytes 2359296 | tf_op jit(solution)/shard_map/all_gather | solution.py:16
  20.9 91.5 %all-gather.6.cloned.1.call-start = ((), (), s32[]{:S(2)}) async-start(), calls=%async_computation.6 | async-start | bytes 2359296 | tf_op jit(solution)/shard_map/all_gather | solution.py:16
  112.4 4.2 %copy-start.2 = (bf16[128,2048]{1,0:T(8,128)(2,1)S(1)}, bf16[128,2048]{1,0:T(8,128)(2,1)}, u32[]{:S(2)}) copy-start(bf16[128,2048]{1,0:T(8,128)(2,1)} %param.21) | copy-start | bytes 1572868
  117.2 8.7 %copy-start.4 = (s32[256,2]{0,1:T(2,128)S(1)}, s32[256,2]{0,1:T(2,128)}, u32[]{:S(2)}) copy-start(s32[256,2]{0,1:T(2,128)} %param.23) | copy-start | bytes 6148
  118.4 33.7 %copy-start.3 = (bf16[256,128]{1,0:T(8,128)(2,1)S(1)}, bf16[256,128]{1,0:T(8,128)(2,1)}, u32[]{:S(2)}) copy-start(bf16[256,128]{1,0:T(8,128)(2,1)} %param.16) | copy-start | bytes 196612
  118.4 33.6 %all-to-all-start = ((bf16[16,256,128]{2,1,0:T(8,128)(2,1)}), bf16[16,256,128]{2,1,0:T(8,128)(2,1)S(1)}, u32[]{:S(2)}, u32[]{:S(2)}) async-start(bf16[16,256,128]{2,1,0:T(8,128)(2,1)} %bitcast.60), calls=%async_computation | async-start | bytes 2097152 | tf_op jit(solution)/shard_map/all_to_all | solution.py:27
  152.9 9.7 %all-to-all-start.1 = ((f32[16,1,256]{2,1,0:T(1,128)}), f32[16,1,256]{2,1,0:T(1,128)S(1)}, u32[]{:S(2)}, u32[]{:S(2)}) async-start(f32[16,1,256]{2,1,0:T(1,128)} %broadcast_in_dim.101), calls=%async_computation.1 | async-start | bytes 32768 | tf_op jit(solution)/shard_map/all_to_all | solution.py:33
  158.1 90.4 %all-gather.8.cloned.1.call-start = ((), (), s32[]{:S(2)}) async-start(), calls=%async_computation.7 | async-start | bytes 3342336 | tf_op jit(solution)/shard_map/all_gather | solution.py:150
  209.2 44.4 %copy-start.6 = (bf16[1,2048,256]{2,1,0:T(8,128)(2,1)S(1)}, bf16[1,2048,256]{2,1,0:T(8,128)(2,1)}, u32[]{:S(2)}) copy-start(bf16[1,2048,256]{2,1,0:T(8,128)(2,1)} %param.25) | copy-start | bytes 3145732
  253.7 2.8 copy-start.1
  253.7 2.8 copy-start.7
  260.5 7.2 %copy-start.5 = (f32[256,2]{0,1:T(2,128)S(1)}, f32[256,2]{0,1:T(2,128)}, u32[]{:S(2)}) copy-start(f32[256,2]{0,1:T(2,128)} %param.24) | copy-start | bytes 6148
  260.5 66.5 %all-to-all-start.3 = ((bf16[16,32,20,128]{3,1,2,0:T(8,128)(2,1)}), bf16[16,32,20,128]{3,1,2,0:T(8,128)(2,1)}, u32[]{:S(2)}, u32[]{:S(2)}) async-start(bf16[16,32,20,128]{3,1,2,0:T(8,128)(2,1)} %bitcast.62), calls=%async_computation.3 | async-start | bytes 5242880 | tf_op jit(solution)/shard_map/all_to_all | solution.py:27
  329.8 21.8 %all-to-all-start.4 = ((bf16[32,20,128]{2,1,0:T(8,128)(2,1)}), bf16[32,20,128]{2,1,0:T(8,128)(2,1)S(1)}, u32[]{:S(2)}, u32[]{:S(2)}) async-start(bf16[32,20,128]{2,1,0:T(8,128)(2,1)} %copy.80), calls=%async_computation.4 | async-start | bytes 393216 | tf_op jit(solution)/shard_map/all_to_all | solution.py:172
Sparse Core Ops, SparseCore 0:
  21.0 47.3 all-gather.3
  70.5 41.8 all-gather.5
  209.3 39.0 all-gather.7
where the time goes:
time: 363 us; the launch traced here: 362 us
  waiting for transfers between devices  174 us (48%)
  blocking collectives  113 us (31%)
  starting transfers between devices  29 us (8%)
  local copies, waits for them, and re-layouts  17.1 us (5%)
  between operations  13.4 us (4%)
  other arithmetic  7.3 us (2%)
  matrix products  6.94 us (2%)
    all_to_all x2, waiting for transfers between devices, sum_at_owner(): lax.all_to_all(cut_along(shard, dim, peers), axis, 0, 0, tiled=True)  82.8 us
    all_gather x4, blocking collectives, gathered_by_axis(): out = lax.all_gather(out, axes[number], axis=dim, tiled=True)  69.1 us
    all_to_all x1, blocking collectives, shards(): lax.all_to_all(taken_rows.reshape(sp_count, capacity, normed.shape[1]), S...  44.1 us
    all_gather x1, waiting for transfers between devices, shards(): lax.all_gather(lax.all_to_all(taken_rows.reshape(sp_count, capacity, norm...  39.2 us
    all_gather x2, waiting for transfers between devices, gathered_by_axis(): out = lax.all_gather(out, axes[number], axis=dim, tiled=True)  36.7 us
    all_to_all x2, starting transfers between devices, sum_at_owner(): lax.all_to_all(cut_along(shard, dim, peers), axis, 0, 0, tiled=True)  13.8 us
    all_to_all x1, waiting for transfers between devices, shards(): lax.all_to_all(summed.astype(jnp.bfloat16), SP, split_axis=0, concat_axis...  11.8 us
    all_to_all x1, starting transfers between devices, shards(): lax.all_to_all(summed.astype(jnp.bfloat16), SP, split_axis=0, concat_axis...  9.92 us
  transfers between devices with their start and end apart: 7, of which 6 were waited for; matrix products, arithmetic and copies ran while one was open for 1% of the time, Pallas kernels for 0%

commit v1 on v0

--- a/solution.py
+++ b/solution.py
@@ -147,17 +147,25 @@
     normed = (local_rows * row_scale[:, None] * local_gain[None, :]).astype(jnp.bfloat16)
     taken_rows = jnp.take(normed, source_row, axis=0)
     taken_rows = jnp.where(filled[:, None], taken_rows, jnp.zeros((), normed.dtype))
-    arrived = lax.all_gather(
+    arrived = jnp.concatenate(
         lax.all_to_all(
-            taken_rows.reshape(sp_count, capacity, normed.shape[1]),
-            SP,
-            split_axis=0,
-            concat_axis=0,
-            tiled=True,
+            jnp.stack(
+                [
+                    lax.all_to_all(
+                        taken_rows.reshape(sp_count, capacity, normed.shape[1]),
+                        SP,
+                        split_axis=0,
+                        concat_axis=0,
+                        tiled=True,
+                    )
+                ]
+                * lax.axis_size("tp")
+            ),
+            "tp",
+            0,
+            0,
         ),
-        "tp",
         axis=2,
-        tiled=True,
     )
     source_count = arrived.shape[0]
     slot_count = arrived.shape[1]

time: 363 us -> 379 us (1.044)
  blocking collectives: 113 us -> 179 us
  waiting for transfers between devices: 174 us -> 135 us
  starting transfers between devices: 29 us -> 22.1 us
    all_to_all x0 -> x1, blocking collectives: none -> 65.6 us  [shards(): lax.all_to_all(jnp.stack([lax.all_to_all(taken_rows.reshape(sp_count, cap...]
    all_gather x1 -> x0, waiting for transfers between devices: 39.2 us -> none  [shards(): lax.all_gather(lax.all_to_all(taken_rows.reshape(sp_count, capacity, norm...]
    all_to_all x1, starting transfers between devices: 9.92 us -> 3.87 us  [shards(): lax.all_to_all(summed.astype(jnp.bfloat16), SP, split_axis=0, concat_axis...]
  transfers between devices with their start and end apart: 7 -> 6, of which waited for: 6 -> 5; matrix products, arithmetic and copies ran while one was open for 1% -> 1% of each run, Pallas kernels for 0% -> 0%
where the time goes in v1:
time: 379 us; the launch traced here: 377 us
  blocking collectives  179 us (47%)
  waiting for transfers between devices  135 us (36%)
  starting transfers between devices  22.1 us (6%)
  local copies, waits for them, and re-layouts  14.5 us (4%)
  between operations  13.7 us (4%)
  other arithmetic  7.3 us (2%)
  matrix products  5.04 us (1%)
    all_to_all x2, waiting for transfers between devices, sum_at_owner(): lax.all_to_all(cut_along(shard, dim, peers), axis, 0, 0, tiled=True)  82.8 us
    all_gather x4, blocking collectives, gathered_by_axis(): out = lax.all_gather(out, axes[number], axis=dim, tiled=True)  69.1 us
    all_to_all x1, blocking collectives, shards(): lax.all_to_all(jnp.stack([lax.all_to_all(taken_rows.reshape(sp_count, cap...  65.6 us
    all_to_all x1, blocking collectives, shards(): lax.all_to_all(taken_rows.reshape(sp_count, capacity, normed.shape[1]), S...  44 us
    all_gather x2, waiting for transfers between devices, gathered_by_axis(): out = lax.all_gather(out, axes[number], axis=dim, tiled=True)  36.7 us
    all_to_all x2, starting transfers between devices, sum_at_owner(): lax.all_to_all(cut_along(shard, dim, peers), axis, 0, 0, tiled=True)  13 us
    all_to_all x1, waiting for transfers between devices, shards(): lax.all_to_all(summed.astype(jnp.bfloat16), SP, split_axis=0, concat_axis...  12.3 us
  transfers between devices with their start and end apart: 6, of which 5 were waited for; matrix products, arithmetic and copies ran while one was open for 1% of the time, Pallas kernels for 0%

profile of v1, /device:TPU:24, one launch (start us, length us, event | category | flops | bytes accessed | tf_op | source)
XLA Modules:
  0.0 377.3 jit_solution(3463351888011368954)
XLA Ops:
  6.5 14.3 %all_gather.18 = bf16[128,1024]{1,0:T(8,128)(2,1)} all-gather(bf16[128,256]{1,0:T(8,128)(2,1)} %param.18), channel_id=1, replica_groups=mesh['sp_0'=8,'sp_1'=4,'tp'=16] {'sp_1'}, dimensions={1}, use_global_device_ids=true | all-gather | bytes 327680 | tf_op jit(solution)/shard_map/all_gather | solution.py:16
  20.9 13.2 %all_gather.22 = bf16[128,1024]{1,0:T(8,128)(2,1)} all-gather(bf16[128,256]{1,0:T(8,128)(2,1)} %param.19), channel_id=1, replica_groups=mesh['sp_0'=8,'sp_1'=4,'tp'=16] {'sp_1'}, dimensions={1}, use_global_device_ids=true | all-gather | bytes 327680 | tf_op jit(solution)/shard_map/all_gather | solution.py:16
  34.2 10.6 %all_gather.20 = f32[2,1024]{1,0:T(2,128)S(1)} all-gather(f32[2,256]{1,0:T(2,128)} %param.20), channel_id=1, replica_groups=mesh['sp_0'=8,'sp_1'=4,'tp'=16] {'sp_1'}, dimensions={1}, use_global_device_ids=true | all-gather | bytes 10240 | tf_op jit(solution)/shard_map/all_gather | solution.py:16
  44.8 31.0 %all_gather.21 = f32[2,8192]{1,0:T(2,128)S(1)} all-gather(f32[2,1024]{1,0:T(2,128)S(1)} %all_gather.20), channel_id=1, replica_groups=mesh['sp_0'=8,'sp_1'=4,'tp'=16] {'sp_0'}, dimensions={1}, use_global_device_ids=true | all-gather | bytes 73728 | tf_op jit(solution)/shard_map/all_gather | solution.py:16
  75.7 36.7 %all-gather.5.cloned.1.call-done = bf16[128,8192]{1,0:T(8,128)(2,1)} async-done(((bf16[128,1024]{1,0:T(8,128)(2,1)}), bf16[128,8192]{1,0:T(8,128)(2,1)}) %all-gather.5.cloned.1.call-update) | async-done | bytes 2097168 | tf_op jit(solution)/shard_map/all_gather | solution.py:16
  112.5 4.2 %while.18 = (s32[]{:T(128)}, f32[2,256]{1,0:T(2,128)S(1)}, f32[2,256]{1,0:T(2,128)S(1)}, f32[2,64,256]{2,1,0:T(8,128)S(1)}, s32[]{:T(128)}, /*index=5*/bf16[128,...) while((s32[]{:T(128)}, f32[2,256]{1,0:T(2,128)S(1)}, ...), condition=%wide.region_5.6_spmd.clone, body=%wide.region_0.5_spmd.clone.sunk | while | flops 139266304 | bytes 8788313 | solution.py:113
  112.5 3.8 %conditional.3 = ((f32[2,256]{1,0:T(2,128)S(1)}, f32[2,256]{1,0:T(2,128)S(1)}, f32[2,64,256]{2,1,0:T(8,128)S(1)})) conditional(s32[]{:T(128)} %convert_element_type.119, (f32[2,256]{1,0:T(2,128)S(1)}, f32[2,256]{1,0:T(2,128)S(1)}, f32[2,64,256]{2,1,0:T(8,128)S(1)}) %tuple.55, (s32[]{:T(128)}, s32[]{:T(128)}, bf16[128,8192]{1,0:T(8,128)(2,1)}, ...), branch_computations={%region_1.0_spmd, %region_2.4_spmd} | conditional | flops 139266304 | bytes 8787026 | solution.py:106
  112.5 1.1 constant_dynamic-slice_fusion
  113.7 0.2 broadcast_compare_fusion
  113.9 1.6 fusion.36
  115.5 0.3 fusion.3
  115.8 0.5 convolution_add_fusion
  116.7 0.5 fusion.13
  117.2 1.3 copy.117
  118.4 7.4 %all-to-all-start = ((bf16[16,256,128]{2,1,0:T(8,128)(2,1)}), bf16[16,256,128]{2,1,0:T(8,128)(2,1)S(1)}, u32[]{:S(2)}, u32[]{:S(2)}) async-start(bf16[16,256,128]{2,1,0:T(8,128)(2,1)} %bitcast.70), calls=%async_computation | async-start | bytes 2097152 | tf_op jit(solution)/shard_map/all_to_all | solution.py:27
  126.0 0.1 eq.39
  126.3 1.2 reduce-window.6
  127.5 0.2 slice_reduce_fusion
  127.8 0.2 select_reduce_fusion
  128.2 0.2 fusion.14
  128.4 23.6 %all-to-all-done = bf16[16,256,128]{2,1,0:T(8,128)(2,1)S(1)} async-done(((bf16[16,256,128]{2,1,0:T(8,128)(2,1)}), bf16[16,256,128]{2,1,0:T(8,128)(2,1)S(1)}, u32[]{:S(2)}, u32[]{:S(2)}) %all-to-all-start) | async-done | bytes 1048608 | tf_op jit(solution)/shard_map/all_to_all | solution.py:27
  152.0 0.1 convert_reduce_fusion
  152.3 0.6 broadcast_in_dim.101
  152.9 5.2 %all-to-all-start.1 = ((f32[16,1,256]{2,1,0:T(1,128)}), f32[16,1,256]{2,1,0:T(1,128)S(1)}, u32[]{:S(2)}, u32[]{:S(2)}) async-start(f32[16,1,256]{2,1,0:T(1,128)} %broadcast_in_dim.101), calls=%async_computation.1 | async-start | bytes 32768 | tf_op jit(solution)/shard_map/all_to_all | solution.py:33
  158.3 0.8 dynamic_slice.42
  159.0 3.6 all-to-all-done.1
  162.8 2.0 gather_fusion
  164.9 0.3 select_select_fusion
  165.1 44.0 %all_to_all.31 = bf16[32,20,128]{2,1,0:T(8,128)(2,1)S(1)} all-to-all(bf16[32,20,128]{2,1,0:T(8,128)(2,1)S(1)} %select_select_fusion), channel_id=1, replica_groups=mesh['sp_0'=8,'sp_1'=4,'tp'=16] {'sp_0','sp_1'}, dimensions={0} | all-to-all | bytes 327680 | tf_op jit(solution)/shard_map/all_to_all | solution.py:154
  209.1 0.5 stack.2
  209.6 65.6 %all_to_all.32 = bf16[16,32,20,128]{3,1,2,0:T(8,128)(2,1)S(1)} all-to-all(bf16[16,32,20,128]{3,1,2,0:T(8,128)(2,1)S(1)} %stack.2), channel_id=1, replica_groups=mesh['sp_0'=8,'sp_1'=4,'tp'=16] {'tp'}, dimensions={0} | all-to-all | bytes 5242880 | tf_op jit(solution)/shard_map/all_to_all | solution.py:151
  275.3 1.7 copy.85
  277.0 0.8 fusion.8
  277.8 0.4 copy-done.6
  278.2 0.9 fusion.18
  279.1 0.8 fusion.12
  280.0 2.2 copy.116
  282.2 5.6 %all-to-all-start.4 = ((bf16[16,32,20,128]{3,1,2,0:T(8,128)(2,1)}), bf16[16,32,20,128]{3,1,2,0:T(8,128)(2,1)}, u32[]{:S(2)}, u32[]{:S(2)}) async-start(bf16[16,32,20,128]{3,1,2,0:T(8,128)(2,1)} %bitcast.72), calls=%async_computation.4 | async-start | bytes 5242880 | tf_op jit(solution)/shard_map/all_to_all | solution.py:27
  288.1 0.1 mul.123
  288.4 0.2 copy.82
  288.7 59.1 %all-to-all-done.4 = bf16[16,32,20,128]{3,1,2,0:T(8,128)(2,1)} async-done(((bf16[16,32,20,128]{3,1,2,0:T(8,128)(2,1)}), bf16[16,32,20,128]{3,1,2,0:T(8,128)(2,1)}, u32[]{:S(2)}, u32[]{:S(2)}) %all-to-all-start.4) | async-done | bytes 2621472 | tf_op jit(solution)/shard_map/all_to_all | solution.py:27
  347.9 2.1 reduce_sum.94
  350.0 0.7 copy.89
  350.7 3.9 %all-to-all-start.5 = ((bf16[32,20,128]{2,1,0:T(8,128)(2,1)}), bf16[32,20,128]{2,1,0:T(8,128)(2,1)S(1)}, u32[]{:S(2)}, u32[]{:S(2)}) async-start(bf16[32,20,128]{2,1,0:T(8,128)(2,1)} %copy.89), calls=%async_computation.5 | async-start | bytes 393216 | tf_op jit(solution)/shard_map/all_to_all | solution.py:180
  354.6 12.3 %all-to-all-done.5 = bf16[32,20,128]{2,1,0:T(8,128)(2,1)S(1)} async-done(((bf16[32,20,128]{2,1,0:T(8,128)(2,1)}), bf16[32,20,128]{2,1,0:T(8,128)(2,1)S(1)}, u32[]{:S(2)}, u32[]{:S(2)}) %all-to-all-start.5) | async-done | bytes 163872 | tf_op jit(solution)/shard_map/all_to_all | solution.py:180
  367.0 1.3 gather_fusion.1
  368.3 1.5 multiply_reduce_fusion
  369.8 0.7 fusion.28
  (71 shorter events, 1.9 us)
Async XLA Ops:
  6.5 272.6 %copy-start = (bf16[1,256,2048]{2,1,0:T(8,128)(2,1)S(1)}, bf16[1,256,2048]{2,1,0:T(8,128)(2,1)}, u32[]{:S(2)}) copy-start(bf16[1,256,2048]{2,1,0:T(8,128)(2,1)} %param.27) | copy-start | bytes 3145732
  6.5 69.2 %all-gather.3.cloned.1.call-start = ((), (), s32[]{:S(2)}) async-start(), calls=%async_computation.6 | async-start | bytes 2359296 | tf_op jit(solution)/shard_map/all_gather | solution.py:16
  20.9 91.5 %all-gather.5.cloned.1.call-start = ((), (), s32[]{:S(2)}) async-start(), calls=%async_computation.7 | async-start | bytes 2359296 | tf_op jit(solution)/shard_map/all_gather | solution.py:16
  112.4 4.2 %copy-start.1 = (bf16[128,2048]{1,0:T(8,128)(2,1)S(1)}, bf16[128,2048]{1,0:T(8,128)(2,1)}, u32[]{:S(2)}) copy-start(bf16[128,2048]{1,0:T(8,128)(2,1)} %param.21) | copy-start | bytes 1572868
  117.2 8.7 %copy-start.3 = (s32[256,2]{0,1:T(2,128)S(1)}, s32[256,2]{0,1:T(2,128)}, u32[]{:S(2)}) copy-start(s32[256,2]{0,1:T(2,128)} %param.23) | copy-start | bytes 6148
  118.4 33.8 %copy-start.2 = (bf16[256,128]{1,0:T(8,128)(2,1)S(1)}, bf16[256,128]{1,0:T(8,128)(2,1)}, u32[]{:S(2)}) copy-start(bf16[256,128]{1,0:T(8,128)(2,1)} %param.16) | copy-start | bytes 196612
  118.4 33.6 %all-to-all-start = ((bf16[16,256,128]{2,1,0:T(8,128)(2,1)}), bf16[16,256,128]{2,1,0:T(8,128)(2,1)S(1)}, u32[]{:S(2)}, u32[]{:S(2)}) async-start(bf16[16,256,128]{2,1,0:T(8,128)(2,1)} %bitcast.70), calls=%async_computation | async-start | bytes 2097152 | tf_op jit(solution)/shard_map/all_to_all | solution.py:27
  152.9 9.7 %all-to-all-start.1 = ((f32[16,1,256]{2,1,0:T(1,128)}), f32[16,1,256]{2,1,0:T(1,128)S(1)}, u32[]{:S(2)}, u32[]{:S(2)}) async-start(f32[16,1,256]{2,1,0:T(1,128)} %broadcast_in_dim.101), calls=%async_computation.1 | async-start | bytes 32768 | tf_op jit(solution)/shard_map/all_to_all | solution.py:33
  275.3 1.7 copy-start.5
  277.0 1.2 copy-start.6
  282.2 6.4 %copy-start.4 = (f32[256,2]{0,1:T(2,128)S(1)}, f32[256,2]{0,1:T(2,128)}, u32[]{:S(2)}) copy-start(f32[256,2]{0,1:T(2,128)} %param.24) | copy-start | bytes 6148
  282.2 65.7 %all-to-all-start.4 = ((bf16[16,32,20,128]{3,1,2,0:T(8,128)(2,1)}), bf16[16,32,20,128]{3,1,2,0:T(8,128)(2,1)}, u32[]{:S(2)}, u32[]{:S(2)}) async-start(bf16[16,32,20,128]{3,1,2,0:T(8,128)(2,1)} %bitcast.72), calls=%async_computation.4 | async-start | bytes 5242880 | tf_op jit(solution)/shard_map/all_to_all | solution.py:27
  350.7 16.2 %all-to-all-start.5 = ((bf16[32,20,128]{2,1,0:T(8,128)(2,1)}), bf16[32,20,128]{2,1,0:T(8,128)(2,1)S(1)}, u32[]{:S(2)}, u32[]{:S(2)}) async-start(bf16[32,20,128]{2,1,0:T(8,128)(2,1)} %copy.89), calls=%async_computation.5 | async-start | bytes 393216 | tf_op jit(solution)/shard_map/all_to_all | solution.py:180
Sparse Core Ops, SparseCore 0:
  21.0 47.3 all-gather.2
  70.5 41.8 all-gather.4
